TPU v7x, 32 devices: a whole 2x2x4 slice. The times are simulated.
32 devices in a mesh: ep: 8 (over z, core), tp: 4 (over y, x).
Axes of the slice: x: 2, y: 2, z: 4, core: 2. Of those that a mesh axis runs over, the one named last changes fastest.
Arguments:
- branch_in: bfloat16 [8192, 512], P(('ep', 'tp')), may hold values from -6 to 6
- pool_weight: bfloat16 [4, 128, 128], replicated, may hold values from -0.5 to 0.5
- group_gain: float32 [512], replicated, may hold values from 0.1 to 1.9
- out_weight: bfloat16 [512, 2048], P(None, 'tp'), may hold values from -0.25 to 0.25
- out_gain: float32 [2048], replicated, may hold values from 0.1 to 1.9
- ffn_input: bfloat16 [1024, 2048], P('ep'), may hold values from -6 to 6
- ffn_gain: float32 [2048], replicated, may hold values from 0.1 to 1.9
- routes: int32 [1024, 4], P('ep'), may hold values from 0 to 7, all different within a row; in each aligned block of 128 rows (0 to 127, 128 to 255, ...) at most 128 rows name the same one
- route_weight: float32 [1024, 4], P('ep'), may hold values from 0.2 to 2
- gate_weight: bfloat16 [8, 2048, 4096], P('ep', None, 'tp'), may hold values from -0.375 to 0.375
- up_weight: bfloat16 [8, 2048, 4096], P('ep', None, 'tp'), may hold values from -0.375 to 0.375
- down_weight: bfloat16 [8, 4096, 2048], P('ep', 'tp'), may hold values from -0.0078125 to 0.0078125
Outputs:
- mixer_out: bfloat16 [8192, 2048], P(('ep', 'tp'))
- expert_out: bfloat16 [1024, 2048], P('ep', 'tp')
Inputs may be any that keep to these rules, and one draw needn't show every extreme that they name: `routes`: each row names 4 different experts. Among the 128 rows of one index of ep no expert is named by more than 128 rows, and in some such block one expert is named by exactly 128.
All inputs are finite; a program needn't handle non-finite values.
Results may differ from a plain program's by a relative error of at most 0.017.
Values may be sent and summed in bfloat16 or wider, within the bound.
A program may use at most 64 MiB of HBM per device.

v0:
```python
import functools
import jax
import jax.numpy as jnp
from jax import lax
from jax.experimental import pallas as pl
from jax.experimental.pallas import tpu as pltpu
from jax.sharding import PartitionSpec as P

pool_windows = (2, 4, 8, 16)
rim_rows = 16
norm_eps = 1e-06
clamp_limit = 7.0
sigmoid_slope = 1.702
MESH = pl.DeviceIdType.MESH
f32 = jnp.float32
bf16 = jnp.bfloat16


def rms_scale(values, gain):
    return values * lax.rsqrt(jnp.mean(values * values, axis=-1, keepdims=True) + norm_eps) * gain


def kernel(
    n_ep, n_tp,
    branch, pool_w, group_gain, out_w, out_gain, x_own, ffn_gain, w_own, gate_h, up_h, down_h,
    mixer_out, expert_out,
    gate, up, down, xg, wg, rim, ow, hid, mixed, proj,
    pown, psend, precv, tsend, trecv, fsend, frecv, facc,
    local_sem, s_z, r_z, s_x, r_x, s_p, r_p, s_w, r_w, s_rim, r_rim,
    s_ow, r_ow, s_owp, r_owp, s_ps, r_ps, s_t, r_t, s_f, r_f,
):
    e = lax.axis_index("ep")
    j = lax.axis_index("tp")
    nz = n_ep // 2
    z = e // 2
    c = e % 2
    rows, width = x_own.shape
    cols = width // n_tp
    mate = z * 2 + (1 - c)
    last = (j == n_tp - 1).astype(jnp.int32)
    first = (j == 0).astype(jnp.int32)
    nxt = ((e + last) % n_ep, (j + 1) % n_tp)
    prv = ((e - first + n_ep) % n_ep, (j - 1 + n_tp) % n_tp)

    def colsl(q):
        return pl.ds(pl.multiple_of(q * cols, cols), cols)

    def remote(src, dst, ssem, rsem, ep, tp):
        return pltpu.make_async_remote_copy(
            src_ref=src, dst_ref=dst, send_sem=ssem, recv_sem=rsem,
            device_id=(ep, tp), device_id_type=MESH,
        )

    def ep_at(d):
        return (z + d) % nz * 2 + c

    def src_ep(d):
        return (z - d + nz) % nz * 2 + c

    def src_mate(d):
        return (z - d + nz) % nz * 2 + (1 - c)

    def tp_at(t):
        return (j + t) % n_tp

    loads = [
        pltpu.make_async_copy(gate_h.at[0], gate, local_sem.at[0]),
        pltpu.make_async_copy(up_h.at[0], up, local_sem.at[1]),
        pltpu.make_async_copy(down_h.at[0], down, local_sem.at[2]),
    ]
    own_w = pltpu.make_async_copy(w_own, wg.at[e], local_sem.at[4])
    own_ow = pltpu.make_async_copy(out_w, ow.at[j], local_sem.at[5])
    own_w.start()
    own_ow.start()
    for load in loads:
        load.start()

    barrier = pltpu.get_barrier_semaphore()
    for d in range(1, n_ep):
        pl.semaphore_signal(barrier, inc=1, device_id=((e + d) % n_ep, j), device_id_type=MESH)
    for t in range(1, n_tp):
        pl.semaphore_signal(barrier, inc=1, device_id=(e, tp_at(t)), device_id_type=MESH)
    pl.semaphore_signal(barrier, inc=1, device_id=nxt, device_id_type=MESH)
    pl.semaphore_signal(barrier, inc=1, device_id=prv, device_id_type=MESH)

    chunk = 16

    def norm_rows(i, _):
        r = pl.ds(pl.multiple_of(i * chunk, chunk), chunk)
        xg[e, r, :] = rms_scale(x_own[r, :].astype(f32), ffn_gain[...]).astype(bf16)
        return 0

    lax.fori_loop(0, rows // chunk, norm_rows, 0)
    pl.semaphore_wait(barrier, n_ep - 1 + n_tp - 1 + 2)

    def z_copy(d):
        return remote(
            xg.at[e, :, colsl(j)], xg.at[e, :, colsl(j)], s_z.at[d], r_z.at[d], ep_at(d), j
        )

    def z_arrival(d):
        view = xg.at[src_ep(d), :, colsl(j)]
        return remote(view, view, s_z.at[d], r_z.at[d], ep_at(d), j)

    def x_copy(d, t):
        view = xg.at[src_ep(d), :, colsl(j)]
        return remote(view, view, s_x.at[d, t], r_x.at[d, t], e, tp_at(t))

    def x_arrival(d, t):
        view = xg.at[src_ep(d), :, colsl(tp_at(n_tp - t))]
        return remote(view, view, s_x.at[d, t], r_x.at[d, t], e, tp_at(t))

    def p_copy(d):
        view = xg.at[src_ep(d)]
        return remote(view, view, s_p.at[d], r_p.at[d], mate, j)

    def p_arrival(d):
        view = xg.at[src_mate(d)]
        return remote(view, view, s_p.at[d], r_p.at[d], mate, j)

    own_p = remote(xg.at[e], xg.at[e], s_p.at[0], r_p.at[0], mate, j)
    half = out_w.shape[0] // 2
    my_half = pl.ds(pl.multiple_of(c * half, half), half)
    mate_half = pl.ds(pl.multiple_of((1 - c) * half, half), half)

    def w_copy(d):
        return remote(w_own, wg.at[e], s_w.at[d], r_w.at[d], (e + d) % n_ep, j)

    def w_arrival(d):
        return remote(w_own, wg.at[(e - d + n_ep) % n_ep], s_w.at[d], r_w.at[d], (e + d) % n_ep, j)

    def ow_copy(t):
        return remote(
            out_w.at[my_half], ow.at[j, my_half], s_ow.at[t], r_ow.at[t], e, tp_at(t)
        )

    def ow_arrival(t):
        view = ow.at[tp_at(n_tp - t), my_half]
        return remote(view, view, s_ow.at[t], r_ow.at[t], e, tp_at(t))

    def owp_copy(t):
        view = ow.at[tp_at(n_tp - t), my_half]
        return remote(view, view, s_owp.at[t], r_owp.at[t], mate, j)

    def owp_arrival(t):
        view = ow.at[tp_at(n_tp - t), mate_half]
        return remote(view, view, s_owp.at[t], r_owp.at[t], mate, j)

    rim_copy = remote(
        branch.at[pl.ds(branch.shape[0] - rim_rows, rim_rows)], rim, s_rim, r_rim, nxt[0], nxt[1]
    )

    for d in range(1, nz):
        z_copy(d).start()
    own_p.start()
    rim_copy.start()
    for d in range(1, n_ep):
        w_copy(d).start()
    for t in range(1, n_tp):
        ow_copy(t).start()

    rim_copy.wait_recv()
    branch_rows = branch.shape[0]
    chans = branch.shape[1] // len(pool_windows)
    first_row = (e * n_tp + j) * branch_rows
    positions = first_row + lax.broadcasted_iota(jnp.int32, (branch_rows, 1), 0)
    total = jnp.zeros((branch_rows, 1), f32)
    for g, window in enumerate(pool_windows):
        lanes = slice(g * chans, (g + 1) * chans)
        here = branch[:, lanes].astype(f32)
        edge = jnp.where(first_row == 0, 0.0, rim[:, lanes].astype(f32))
        wide = jnp.concatenate([edge, here], axis=0)
        reach = 1
        while reach < window:
            wide = wide + pltpu.roll(wide, reach, 0)
            reach *= 2
        counts = jnp.minimum(window, positions + 1).astype(f32)
        pooled = (wide[rim_rows:] / counts - here).astype(bf16)
        part = jnp.dot(pooled, pool_w[g], preferred_element_type=f32)
        proj[:, lanes] = part
        total = total + jnp.sum(part * part, axis=-1, keepdims=True)
    scale = lax.rsqrt(total / branch.shape[1] + norm_eps)
    mixed[...] = (proj[:, : branch.shape[1]] * scale * group_gain[...]).astype(bf16)

    def forward(d):
        z_arrival(d).wait_recv()
        for t in range(1, n_tp):
            x_copy(d, t).start()

    def to_mate(d):
        for t in range(1, n_tp):
            x_arrival(d, t).wait_recv()
        p_copy(d).start()

    if nz > 1:
        forward(1)
    own_w.wait()
    own_ow.wait()
    for d in range(1, n_ep):
        w_arrival(d).wait_recv()
    for load in loads[:2]:
        load.wait()

    diagonal = lax.broadcasted_iota(jnp.int32, (rows, rows), 0) == lax.broadcasted_iota(
        jnp.int32, (rows, rows), 1
    )

    def row_weights(block):
        line = wg[block, pl.ds(e, 1), :]
        return jnp.sum(jnp.where(diagonal, line, 0.0), axis=1, keepdims=True)

    step_f = min(512, gate.shape[1])

    def hidden_part(s):
        def one(n, _):
            span = pl.ds(pl.multiple_of(n * step_f, step_f), step_f)
            both = jnp.concatenate([xg[src_ep(s)], xg[src_mate(s)]], axis=0)
            g = jnp.dot(both, gate[:, span], preferred_element_type=f32)
            u = jnp.dot(both, up[:, span], preferred_element_type=f32)
            g = jnp.minimum(g, clamp_limit)
            u = jnp.clip(u, -clamp_limit, clamp_limit)
            hid[:, span] = ((u + 1.0) * g * jax.nn.sigmoid(sigmoid_slope * g)).astype(bf16)
            return 0

        lax.fori_loop(0, gate.shape[1] // step_f, one, 0)

    step_d = min(512, width)

    def down_part(s):
        mine = row_weights(src_ep(s))
        theirs = row_weights(src_mate(s))

        def one(q, _):
            span = pl.ds(pl.multiple_of(q * step_d, step_d), step_d)
            y = jnp.dot(hid[...], down[:, span], preferred_element_type=f32)
            pown[s % 2, :, span] = y[:rows] * mine
            psend[s, :, span] = (y[rows:] * theirs).astype(bf16)
            return 0

        lax.fori_loop(0, width // step_d, one, 0)

    def mate_sum(s):
        return remote(psend.at[s], precv.at[s], s_ps.at[s], r_ps.at[s], mate, j)

    def t_copy(s, t):
        return remote(
            tsend.at[s, :, colsl(tp_at(t))], trecv.at[s, t], s_t.at[s, t], r_t.at[s, t], e, tp_at(t)
        )

    def f_copy(s):
        return remote(fsend.at[s], frecv.at[s], s_f.at[s], r_f.at[s], src_ep(s), j)

    def stage_two(s):
        mate_sum(s).wait_recv()

        def one(i, _):
            r = pl.ds(pl.multiple_of(i * chunk, chunk), chunk)
            tsend[s, r, :] = (pown[s % 2, r, :] + precv[s, r, :].astype(f32)).astype(bf16)
            return 0

        lax.fori_loop(0, rows // chunk, one, 0)
        for t in range(1, n_tp):
            t_copy(s, t).start()

    def stage_three(s):
        for t in range(1, n_tp):
            t_copy(s, t).wait_recv()
        acc = tsend[s, :, colsl(j)].astype(f32)
        for t in range(1, n_tp):
            acc = acc + trecv[s, t].astype(f32)

        @pl.when(s == 0)
        def _():
            facc[...] = acc

        @pl.when(s > 0)
        def _():
            fsend[s] = acc.astype(bf16)
            f_copy(s).start()

    def project():
        for t in range(1, n_tp):
            owp_arrival(t).wait_recv()

        def one(q, total):
            part = jnp.dot(mixed[...], ow[q], preferred_element_type=f32)
            proj[:, colsl(q)] = part
            return total + jnp.sum(part * part, axis=-1, keepdims=True)

        total = lax.fori_loop(0, n_tp, one, jnp.zeros((branch_rows, 1), f32))
        scale = lax.rsqrt(total / width + norm_eps)

        def two(q, _):
            mixer_out[:, colsl(q)] = (proj[:, colsl(q)] * scale * out_gain[:, colsl(q)]).astype(bf16)
            return 0

        lax.fori_loop(0, n_tp, two, 0)

    def step(s, _):
        @pl.when(s < nz)
        def _():
            @pl.when(s == 0)
            def _():
                own_arr = remote(xg.at[mate], xg.at[mate], s_p.at[0], r_p.at[0], mate, j)
                own_arr.wait_recv()

            @pl.when(s > 0)
            def _():
                p_arrival(s).wait_recv()

            @pl.when(s + 2 < nz)
            def _():
                forward(s + 2)

            hidden_part(s)

        @pl.when((s > 0) & (s <= nz))
        def _():
            stage_two(s - 1)

        @pl.when(s < nz)
        def _():
            @pl.when(s == 0)
            def _():
                loads[2].wait()

            down_part(s)
            mate_sum(s).start()

            @pl.when(s + 1 < nz)
            def _():
                to_mate(s + 1)

        @pl.when(s == 0)
        def _():
            for t in range(1, n_tp):
                ow_arrival(t).wait_recv()
                owp_copy(t).start()

        @pl.when(s == nz)
        def _():
            project()

        @pl.when(s > 1)
        def _():
            stage_three(s - 2)

        return 0

    lax.fori_loop(0, nz + 2, step, 0)

    acc = facc[...]
    for d in range(1, nz):
        f_copy(d).wait_recv()
        acc = acc + frecv[d].astype(f32)
    expert_out[...] = acc.astype(bf16)

    own_p.wait_send()
    rim_copy.wait_send()
    for d in range(1, n_ep):
        w_copy(d).wait_send()
    for t in range(1, n_tp):
        ow_copy(t).wait_send()
        owp_copy(t).wait_send()

    def drain(s, _):
        mate_sum(s).wait_send()
        for t in range(1, n_tp):
            t_copy(s, t).wait_send()

        @pl.when(s > 0)
        def _():
            z_copy(s).wait_send()
            p_copy(s).wait_send()
            f_copy(s).wait_send()
            for t in range(1, n_tp):
                x_copy(s, t).wait_send()

        return 0

    lax.fori_loop(0, nz, drain, 0)


def per_device(
    n_ep, n_tp,
    branch_in, pool_weight, group_gain, out_weight, out_gain,
    ffn_input, ffn_gain, routes, route_weight, gate_weight, up_weight, down_weight,
):
    rows, width = ffn_input.shape
    nz = n_ep // 2
    cols = width // n_tp
    hidden = gate_weight.shape[2]
    branch_rows, branch_width = branch_in.shape
    named = routes[None, :, :] == jnp.arange(n_ep, dtype=jnp.int32)[:, None, None]
    w_own = jnp.sum(jnp.where(named, route_weight[None, :, :], 0.0), axis=2)
    vm = pl.BlockSpec(memory_space=pltpu.VMEM)
    anyspace = pl.BlockSpec(memory_space=pl.ANY)
    dma = pltpu.SemaphoreType.DMA
    return pl.pallas_call(
        functools.partial(kernel, n_ep, n_tp),
        out_shape=(
            jax.ShapeDtypeStruct((branch_rows, width), bf16),
            jax.ShapeDtypeStruct((rows, cols), bf16),
        ),
        in_specs=[vm] * 8 + [anyspace] * 3,
        out_specs=(vm, vm),
        scratch_shapes=[
            pltpu.VMEM((width, hidden), bf16),
            pltpu.VMEM((width, hidden), bf16),
            pltpu.VMEM((hidden, width), bf16),
            pltpu.VMEM((n_ep, rows, width), bf16),
            pltpu.VMEM((n_ep, n_ep, rows), f32),
            pltpu.VMEM((rim_rows, branch_width), bf16),
            pltpu.VMEM((n_tp, branch_width, cols), bf16),
            pltpu.VMEM((2 * rows, hidden), bf16),
            pltpu.VMEM((branch_rows, branch_width), bf16),
            pltpu.VMEM((branch_rows, width), f32),
            pltpu.VMEM((2, rows, width), f32),
            pltpu.VMEM((nz, rows, width), bf16),
            pltpu.VMEM((nz, rows, width), bf16),
            pltpu.VMEM((nz, rows, width), bf16),
            pltpu.VMEM((nz, n_tp, rows, cols), bf16),
            pltpu.VMEM((nz, rows, cols), bf16),
            pltpu.VMEM((nz, rows, cols), bf16),
            pltpu.VMEM((rows, cols), f32),
            dma((6,)),
            dma((nz,)), dma((nz,)),
            dma((nz, n_tp)), dma((nz, n_tp)),
            dma((nz,)), dma((nz,)),
            dma((n_ep,)), dma((n_ep,)),
            dma, dma,
            dma((n_tp,)), dma((n_tp,)),
            dma((n_tp,)), dma((n_tp,)),
            dma((nz,)), dma((nz,)),
            dma((nz, n_tp)), dma((nz, n_tp)),
            dma((nz,)), dma((nz,)),
        ],
        compiler_params=pltpu.CompilerParams(
            collective_id=0, has_side_effects=True, vmem_limit_bytes=67043328
        ),
    )(
        branch_in, pool_weight, group_gain.reshape(1, -1), out_weight, out_gain.reshape(1, -1),
        ffn_input, ffn_gain.reshape(1, -1), w_own, gate_weight, up_weight, down_weight,
    )


def solution(mesh):
    in_specs = (
        P(("ep", "tp"), None),
        P(),
        P(),
        P(None, "tp"),
        P(),
        P("ep", None),
        P(),
        P("ep", None),
        P("ep", None),
        P("ep", None, "tp"),
        P("ep", None, "tp"),
        P("ep", "tp", None),
    )
    out_specs = (P(("ep", "tp"), None), P("ep", "tp"))
    return jax.shard_map(
        functools.partial(per_device, mesh.shape["ep"], mesh.shape["tp"]),
        mesh=mesh, in_specs=in_specs, out_specs=out_specs, check_vma=False,
    )
```

profile of v0, /device:TPU:0, one launch (start us, length us, event | category | flops | bytes accessed | tf_op | source)
XLA Modules:
  0.0 72.9 jit_solution(12522479872014948391)
XLA Ops:
  0.6 1.3 %select_reduce_fusion.w_own = f32[8,128]{1,0:T(8,128)} fusion(f32[128,4]{0,1:T(4,128)} %param.20, s32[128,4]{0,1:T(4,128)} %param.19), kind=kLoop, calls=%fused_computation | loop fusion | flops 11264 | bytes 8192 | tf_op jit(solution)/shard_map/reduce_sum | solution.py:395
  1.9 67.1 %shard_map.131 = (bf16[256,2048]{1,0:T(8,128)(2,1)}, bf16[128,512]{1,0:T(8,128)(2,1)}) custom-call(bf16[256,512]{1,0:T(8,128)(2,1)} %branch.1, bf16[4,128,128]{2,1,0:T(8,128)(2,1)} %pool_w.1, f32[1,512]{1,0:T(1,128)} %bitcast.5, bf16[512,512]{1,0:T(8,128)(2,1)} %out_w.1, f32[1,2048]{1,0:T(1,128)} %bitcast.3, bf16[128,2048]{1,0:T(8,128)(2,1)} %x_own.1, ...), custom_call_target="tpu_custom_call" | custom-call | tf_op jit(solution)/shard_map/pallas_call | solution.py:399
  69.1 2.3 %copy.18 = bf16[256,2048]{1,0:T(8,128)(2,1)} copy(bf16[256,2048]{1,0:T(8,128)(2,1)} %get-tuple-element.4) | data formatting | bytes 2097152
  71.4 1.6 %copy.19 = bf16[128,512]{1,0:T(8,128)(2,1)} copy(bf16[128,512]{1,0:T(8,128)(2,1)} %get-tuple-element.5) | data formatting | bytes 262144
where the time goes:
time: 73.2 us; the launch traced here: 72.9 us
  Pallas kernels  67.1 us (92%)
  local copies, waits for them, and re-layouts  3.87 us (5%)
  other arithmetic  1.3 us (2%)
    pallas_call x1, Pallas kernels, per_device(): pl.pallas_call(functools.partial(kernel, n_ep, n_tp), out_shape=(jax.Shap...  67.1 us
    unnamed x2, local copies, waits for them, and re-layouts  3.87 us

commit v1 on v0

v1 whole, which is shorter than its diff:
```python
import functools
import math
import jax
import jax.numpy as jnp
from jax import lax
from jax.experimental import pallas as pl
from jax.experimental.pallas import tpu as pltpu
from jax.sharding import PartitionSpec as P

pool_windows = (2, 4, 8, 16)
rim_rows = 16
norm_eps = 1e-06
clamp_limit = 7.0
sigmoid_slope = 1.702
MESH = pl.DeviceIdType.MESH
f32 = jnp.float32
bf16 = jnp.bfloat16


def rms_scale(values, gain):
    return values * lax.rsqrt(jnp.mean(values * values, axis=-1, keepdims=True) + norm_eps) * gain


def grid_of(n_tp):
    nx = 1
    for k in range(1, n_tp + 1):
        if n_tp % k == 0 and k * k <= n_tp:
            nx = k
    return n_tp // nx, nx


def kernel(
    n_ep, n_tp,
    group_gain, out_gain, ffn_gain, routes, route_w, branch_h, pool_h, out_w, x_h, gate_h, up_h, down_h,
    mixer_h, expert_h,
    branch, pool_w, x_own, gate, up, down, xg, wg, rim, ow, hid, mixed, proj, mixer_out, expert_out,
    pown, psend, precv, ts_a, ts_b, t1, u2, t2, fsend, frecv, facc,
    local_sem, sent, r_z, r_x1, r_x2, r_p, r_m, r_t1, r_t2, r_one,
):
    e = lax.axis_index("ep")
    j = lax.axis_index("tp")
    nz = n_ep // 2
    ny, nx = grid_of(n_tp)
    z = e // 2
    c = e % 2
    y = j // nx
    x = j % nx
    rows, width = x_own.shape
    cols = width // n_tp
    half = rows // 2
    qr = rows // 4
    upper = pl.ds(0, half)
    lower = pl.ds(half, half)
    mate = z * 2 + (1 - c)
    last = (j == n_tp - 1).astype(jnp.int32)
    first = (j == 0).astype(jnp.int32)
    nxt = ((e + last) % n_ep, (j + 1) % n_tp)
    prv = ((e - first + n_ep) % n_ep, (j - 1 + n_tp) % n_tp)
    paired = nz & (nz - 1) == 0
    S_Z, S_X1, S_X2, S_P, S_W, S_RIM, S_O, S_O2, S_OP, S_M, S_T1, S_T2, S_F = range(13)
    R_W, R_RIM, R_OA, R_OB, R_O2, R_OP, R_F = range(7)

    def hop(s):
        return (nz - s) % nz

    def partner(s, sign):
        s = hop(s)
        if not paired:
            return (z + sign * s + nz) % nz
        total, bit = 0, 1
        while bit < nz:
            total = total + (z // bit + s // bit) % 2 * bit
            bit *= 2
        return total

    def ep_at(d):
        return partner(d, 1) * 2 + c

    def src_ep(d):
        return partner(d, -1) * 2 + c

    def src_mate(d):
        return partner(d, -1) * 2 + (1 - c)

    def at(dy, dx):
        return (y + dy + ny) % ny * nx + (x + dx + nx) % nx

    def colsl(q):
        return pl.ds(pl.multiple_of(q * cols, cols), cols)

    def send(src, dst, kind, rsem, ep, tp):
        pltpu.make_async_remote_copy(
            src_ref=src, dst_ref=dst, send_sem=sent.at[kind], recv_sem=rsem,
            device_id=(ep, tp), device_id_type=MESH,
        ).start()

    def landed(view, sem):
        pltpu.make_async_copy(view, view, sem).wait()

    steps_x = range(1, nx)
    steps_y = range(1, ny)
    near = nx + ny - 2
    far = (nx - 1) * (ny - 1)

    barrier = pltpu.get_barrier_semaphore()
    for d in range(1, n_ep):
        pl.semaphore_signal(barrier, inc=1, device_id=((e + d) % n_ep, j), device_id_type=MESH)
    for t in range(1, n_tp):
        pl.semaphore_signal(barrier, inc=1, device_id=(e, (j + t) % n_tp), device_id_type=MESH)
    pl.semaphore_signal(barrier, inc=1, device_id=nxt, device_id_type=MESH)
    pl.semaphore_signal(barrier, inc=1, device_id=prv, device_id_type=MESH)

    load_x = pltpu.make_async_copy(x_h, x_own, local_sem.at[0])
    load_branch = pltpu.make_async_copy(branch_h, branch, local_sem.at[1])
    own_ow = pltpu.make_async_copy(out_w, ow.at[j], local_sem.at[2])
    load_pool = pltpu.make_async_copy(pool_h, pool_w, local_sem.at[3])
    loads = [
        pltpu.make_async_copy(gate_h.at[0], gate, local_sem.at[4]),
        pltpu.make_async_copy(up_h.at[0], up, local_sem.at[5]),
        pltpu.make_async_copy(down_h.at[0], down, local_sem.at[6]),
    ]
    write_mixer = pltpu.make_async_copy(mixer_out, mixer_h, local_sem.at[7])
    write_expert = pltpu.make_async_copy(expert_out, expert_h, local_sem.at[8])
    for load in [load_x, load_branch, own_ow, load_pool] + loads:
        load.start()

    chunk = 16

    def norm_rows(i, _):
        r = pl.ds(pl.multiple_of(i * chunk, chunk), chunk)
        xg[e, r, :] = rms_scale(x_own[r, :].astype(f32), ffn_gain[...]).astype(bf16)
        return 0

    experts = lax.broadcasted_iota(jnp.int32, (n_ep, rows), 0)
    named = jnp.zeros((n_ep, rows), f32)
    for k in range(routes.shape[0]):
        named = named + jnp.where(routes[pl.ds(k, 1), :] == experts, route_w[pl.ds(k, 1), :], 0.0)
    wg[e] = named

    def norm_part():
        load_x.wait()
        lax.fori_loop(0, rows // chunk, norm_rows, 0)

    def barrier_wait():
        pl.semaphore_wait(barrier, n_ep - 1 + n_tp - 1 + 2)

    norm_part()
    barrier_wait()

    quart = out_w.shape[0] // 4
    ow_rows = [pl.ds(pl.multiple_of((c * 2 + k) * quart, quart), quart) for k in range(2)]
    my_half = pl.ds(pl.multiple_of(c * 2 * quart, quart), 2 * quart)

    def ow_own(k):
        mine = ow.at[j, ow_rows[k]]
        for dx in steps_x:
            send(mine, mine, S_O, r_one.at[R_OA + k], e, at(0, dx))
        mine = ow.at[j, ow_rows[1 - k]]
        for dy in steps_y:
            send(mine, mine, S_O, r_one.at[R_OA + k], e, at(dy, 0))

    def ow_relay():
        landed(ow.at[pl.ds(0, near), pl.ds(0, quart)], r_one.at[R_OA])
        for dx in steps_x:
            view = ow.at[at(0, -dx), ow_rows[0]]
            for dy in steps_y:
                send(view, view, S_O2, r_one.at[R_O2], e, at(dy, 0))
        for dy in steps_y:
            view = ow.at[at(-dy, 0), ow_rows[1]]
            for dx in steps_x:
                send(view, view, S_O2, r_one.at[R_O2], e, at(0, dx))

    def ow_to_mate():
        landed(ow.at[pl.ds(0, near), pl.ds(0, quart)], r_one.at[R_OB])
        landed(ow.at[pl.ds(0, far), pl.ds(0, 2 * quart)], r_one.at[R_O2])
        for t in range(1, n_tp):
            view = ow.at[(j + t) % n_tp, my_half]
            send(view, view, S_OP, r_one.at[R_OP], mate, j)

    def to_mate(d):
        if not (isinstance(d, int) and d == 0):
            landed(xg.at[0, :, pl.ds(0, far * cols)], r_x2.at[d])
        view = xg.at[src_ep(d)]
        send(view, view, S_P, r_p.at[d], mate, j)

    def start_sends():
        load_branch.wait()
        tail = branch.at[pl.ds(branch.shape[0] - rim_rows, rim_rows)]
        send(tail, rim, S_RIM, r_one.at[R_RIM], nxt[0], nxt[1])
        for d in range(1, n_ep):
            send(wg.at[e], wg.at[e], S_W, r_one.at[R_W], (e + d) % n_ep, j)
        for d in [1, nz - 1] + list(range(2, nz - 1)):
            view = xg.at[e, :, colsl(j)]
            send(view, view, S_Z, r_z.at[d], ep_at(d), j)
        to_mate(0)
        own_ow.wait()
        ow_own(0)
        ow_own(1)

    start_sends()

    branch_rows = branch.shape[0]

    def pool():
        load_pool.wait()
        landed(rim, r_one.at[R_RIM])
        chans = branch.shape[1] // len(pool_windows)
        first_row = (e * n_tp + j) * branch_rows
        positions = first_row + lax.broadcasted_iota(jnp.int32, (branch_rows, 1), 0)
        total = jnp.zeros((branch_rows, 1), f32)
        for g, window in enumerate(pool_windows):
            lanes = slice(g * chans, (g + 1) * chans)
            here = branch[:, lanes].astype(f32)
            edge = jnp.where(first_row == 0, 0.0, rim[:, lanes].astype(f32))
            wide = jnp.concatenate([edge, here], axis=0)
            reach = 1
            while reach < window:
                wide = wide + pltpu.roll(wide, reach, 0)
                reach *= 2
            counts = jnp.minimum(window, positions + 1).astype(f32)
            pooled = (wide[rim_rows:] / counts - here).astype(bf16)
            part = jnp.dot(pooled, pool_w[g], preferred_element_type=f32)
            proj[:, lanes] = part
            total = total + jnp.sum(part * part, axis=-1, keepdims=True)
        scale = lax.rsqrt(total / branch.shape[1] + norm_eps)
        mixed[...] = (proj[:, : branch.shape[1]] * scale * group_gain[...]).astype(bf16)

    def gather_one(d):
        view = xg.at[src_ep(d), :, colsl(j)]
        landed(view, r_z.at[d])
        for dx in steps_x:
            send(view, view, S_X1, r_x1.at[d], e, at(0, dx))
        for dy in steps_y:
            send(view, view, S_X1, r_x1.at[d], e, at(dy, 0))

    def gather_two(d):
        landed(xg.at[0, :, pl.ds(0, near * cols)], r_x1.at[d])
        for dx in steps_x:
            view = xg.at[src_ep(d), upper, colsl(at(0, -dx))]
            for dy in steps_y:
                send(view, view, S_X2, r_x2.at[d], e, at(dy, 0))
        for dy in steps_y:
            view = xg.at[src_ep(d), lower, colsl(at(-dy, 0))]
            for dx in steps_x:
                send(view, view, S_X2, r_x2.at[d], e, at(0, dx))

    diagonal = lax.broadcasted_iota(jnp.int32, (rows, rows), 0) == lax.broadcasted_iota(
        jnp.int32, (rows, rows), 1
    )

    def row_weights(block):
        line = wg[block, pl.ds(e, 1), :]
        return jnp.sum(jnp.where(diagonal, line, 0.0), axis=1, keepdims=True)

    step_f = min(512, gate.shape[1])
    parts_f = gate.shape[1] // step_f

    def hidden_part(s, n):
        span = pl.ds(n * step_f, step_f)
        both = jnp.concatenate([xg[src_ep(s)], xg[src_mate(s)]], axis=0)
        g = jnp.dot(both, gate[:, span], preferred_element_type=f32)
        u = jnp.dot(both, up[:, span], preferred_element_type=f32)
        g = jnp.minimum(g, clamp_limit)
        u = jnp.clip(u, -clamp_limit, clamp_limit)
        hid[:, span] = ((u + 1.0) * g * jax.nn.sigmoid(sigmoid_slope * g)).astype(bf16)

    step_d = min(1024, width)

    def down_part(s):
        mine = row_weights(src_ep(s))
        theirs = row_weights(src_mate(s))

        def one(q, _):
            span = pl.ds(pl.multiple_of(q * step_d, step_d), step_d)
            out = jnp.dot(hid[...], down[:, span], preferred_element_type=f32)
            psend[s, :, span] = (out[rows:] * theirs).astype(bf16)
            pown[s % 2, :, span] = out[:rows] * mine
            send(psend.at[s, :, span], precv.at[s, :, span], S_M, r_m.at[s], mate, j)
            return 0

        lax.fori_loop(0, width // step_d, one, 0)

    def scatter_one(s, h):
        if h == 0:
            landed(precv.at[s], r_m.at[s])
        top = pl.ds(2 * h * qr, qr)
        low = pl.ds((2 * h + 1) * qr, qr)

        def one(q, _):
            a = pown[s % 2, top, colsl(q)] + precv[s, top, colsl(q)].astype(f32)
            b = pown[s % 2, low, colsl(q)] + precv[s, low, colsl(q)].astype(f32)
            ts_a[s, h, q % nx, q // nx] = a.astype(bf16)
            ts_b[s, h, q // nx, q % nx] = b.astype(bf16)
            return 0

        lax.fori_loop(0, n_tp, one, 0)
        for dx in steps_x:
            dst = t1.at[s, h, pl.ds((dx - 1) * ny, ny)]
            send(ts_a.at[s, h, (x + dx) % nx], dst, S_T1, r_t1.at[s, h], e, at(0, dx))
        for dy in steps_y:
            dst = t1.at[s, h, pl.ds((nx - 1) * ny + (dy - 1) * nx, nx)]
            send(ts_b.at[s, h, (y + dy) % ny], dst, S_T1, r_t1.at[s, h], e, at(dy, 0))

    def scatter_two(s, h):
        landed(t1.at[s, h], r_t1.at[s, h])
        for k in range(ny):
            acc = ts_a[s, h, x, k].astype(f32)
            for dx in steps_x:
                acc = acc + t1[s, h, (dx - 1) * ny + k].astype(f32)
            u2[s, h, k] = acc.astype(bf16)
        for k in range(nx):
            acc = ts_b[s, h, y, k].astype(f32)
            for dy in steps_y:
                acc = acc + t1[s, h, (nx - 1) * ny + (dy - 1) * nx + k].astype(f32)
            u2[s, h, ny + k] = acc.astype(bf16)
        for dy in steps_y:
            send(u2.at[s, h, (y + dy) % ny], t2.at[s, h, dy - 1], S_T2, r_t2.at[s, h], e, at(dy, 0))
        for dx in steps_x:
            dst = t2.at[s, h, ny - 1 + dx - 1]
            send(u2.at[s, h, ny + (x + dx) % nx], dst, S_T2, r_t2.at[s, h], e, at(0, dx))

    def scatter_end(s, h):
        landed(t2.at[s, h], r_t2.at[s, h])
        a = u2[s, h, y].astype(f32)
        for dy in steps_y:
            a = a + t2[s, h, dy - 1].astype(f32)
        b = u2[s, h, ny + x].astype(f32)
        for dx in steps_x:
            b = b + t2[s, h, ny - 1 + dx - 1].astype(f32)
        top = pl.ds(2 * h * qr, qr)
        low = pl.ds((2 * h + 1) * qr, qr)
        if isinstance(s, int) and s == 0:
            facc[top] = a
            facc[low] = b
        else:
            fsend[s, top] = a.astype(bf16)
            fsend[s, low] = b.astype(bf16)
            part = pl.ds(2 * h * qr, 2 * qr)
            send(fsend.at[s, part], frecv.at[s, part], S_F, r_one.at[R_F], src_ep(s), j)

    def project():
        landed(ow.at[pl.ds(0, n_tp - 1), pl.ds(0, 2 * quart)], r_one.at[R_OP])

        def one(q, total):
            part = jnp.dot(mixed[...], ow[q], preferred_element_type=f32)
            proj[:, colsl(q)] = part
            return total + jnp.sum(part * part, axis=-1, keepdims=True)

        total = lax.fori_loop(0, n_tp, one, jnp.zeros((branch_rows, 1), f32))
        scale = lax.rsqrt(total / width + norm_eps)

        def two(q, _):
            mixer_out[:, colsl(q)] = (proj[:, colsl(q)] * scale * out_gain[:, colsl(q)]).astype(bf16)
            return 0

        lax.fori_loop(0, n_tp, two, 0)
        write_mixer.start()

    def wait_block(s):
        landed(xg.at[0], r_p.at[s])

    def wait_first():
        for load in loads[:2]:
            load.wait()

    def wait_down():
        loads[2].wait()
        landed(wg.at[pl.ds(0, n_ep - 1)], r_one.at[R_W])

    G1, G2, TM, S1, S2, S3 = gather_one, gather_two, to_mate, scatter_one, scatter_two, scatter_end
    end = nz - 1
    plan = {
        0: (
            [(wait_first,)],
            [],
            [(wait_down,)],
            [(ow_relay,), (pool,), (G1, 1), (G2, 1), (G1, 2), (G1, 3), (TM, 1)],
        ),
        1: ([], [(G2, 2)], [], [(G2, 3), (S1, 1, 0), (S1, 1, 1), (TM, 2)]),
        2: ([], [(TM, 3), (S1, 0, 0)], [(S2, 1, 0), (S1, 0, 1)], [(S2, 1, 1)]),
        end: (
            [],
            [(S1, end - 1, 0), (ow_to_mate,), (S3, end - 2, 0)],
            [(S1, end - 1, 1)],
            [
                (S3, end - 2, 1), (S2, end - 1, 0), (S1, end, 0), (S2, end - 1, 1), (S1, end, 1),
                (S3, end - 1, 0), (project,), (S2, end, 0), (S2, 0, 0), (S3, end - 1, 1), (S2, 0, 1),
                (S2, end, 1), (S3, end, 0), (S3, 0, 0), (S3, end, 1), (S3, 0, 1),
            ],
        ),
    }
    assert nz >= 4

    def middle(s, slot):
        if slot == 1:
            to_mate(s + 1)
            scatter_one(s - 1, 0)
            scatter_end(s - 2, 0)
        if slot == 2:
            scatter_one(s - 1, 1)
        if slot == 3:
            scatter_end(s - 2, 1)
            scatter_two(s - 1, 0)
            scatter_two(s - 1, 1)

    def run(s, slot):
        for i, slots in plan.items():
            if slots[slot]:
                @pl.when(s == i)
                def _():
                    for act in slots[slot]:
                        act[0](*act[1:])

        if nz > 4:
            if slot > 0:
                @pl.when((s > 2) & (s < end))
                def _():
                    middle(s, slot)

            if slot == 3:
                @pl.when((s > 1) & (s + 2 < nz))
                def _():
                    gather_one(s + 2)
                    gather_two(s + 2)

    def step(s, _):
        run(s, 0)
        wait_block(s)
        for n in range(parts_f):
            hidden_part(s, n)
            if n == 0:
                run(s, 1)
        run(s, 2)
        down_part(s)
        run(s, 3)
        return 0

    lax.fori_loop(0, nz, step, 0)

    def drain_all():
        write_mixer.wait()
        landed(fsend.at[pl.ds(1, nz - 1)], sent.at[S_Z])
        landed(xg.at[pl.ds(0, nz - 1), :, pl.ds(0, near * cols)], sent.at[S_X1])
        landed(xg.at[pl.ds(0, nz - 1), :, pl.ds(0, far * cols)], sent.at[S_X2])
        landed(psend, sent.at[S_P])
        landed(wg.at[pl.ds(0, n_ep - 1)], sent.at[S_W])
        landed(rim, sent.at[S_RIM])
        landed(ow.at[pl.ds(0, near), pl.ds(0, 2 * quart)], sent.at[S_O])
        landed(ow.at[pl.ds(0, far), pl.ds(0, 2 * quart)], sent.at[S_O2])
        landed(ow.at[pl.ds(0, n_tp - 1), pl.ds(0, 2 * quart)], sent.at[S_OP])
        landed(psend, sent.at[S_M])
        landed(t1, sent.at[S_T1])
        landed(t2, sent.at[S_T2])

    def final_sum():
        landed(frecv.at[pl.ds(1, nz - 1)], r_one.at[R_F])
        acc = facc[...]
        for d in range(1, nz):
            acc = acc + frecv[d].astype(f32)
        expert_out[...] = acc.astype(bf16)

    def finish():
        write_expert.start()
        landed(fsend.at[pl.ds(1, nz - 1)], sent.at[S_F])
        write_expert.wait()

    drain_all()
    final_sum()
    finish()


def per_device(
    n_ep, n_tp,
    branch_in, pool_weight, group_gain, out_weight, out_gain,
    ffn_input, ffn_gain, routes, route_weight, gate_weight, up_weight, down_weight,
):
    rows, width = ffn_input.shape
    nz = n_ep // 2
    ny, nx = grid_of(n_tp)
    cols = width // n_tp
    qr = rows // 4
    hidden = gate_weight.shape[2]
    branch_rows, branch_width = branch_in.shape
    vm = pl.BlockSpec(memory_space=pltpu.VMEM)
    hbm = pl.BlockSpec(memory_space=pltpu.HBM)
    anyspace = pl.BlockSpec(memory_space=pl.ANY)
    dma = pltpu.SemaphoreType.DMA
    k1 = (nx - 1) * ny + (ny - 1) * nx
    k2 = nx + ny - 2
    buffers = [
        ((branch_rows, branch_width), bf16),
        (pool_weight.shape, bf16),
        ((rows, width), bf16),
        ((width, hidden), bf16),
        ((width, hidden), bf16),
        ((hidden, width), bf16),
        ((n_ep, rows, width), bf16),
        ((n_ep, n_ep, rows), f32),
        ((rim_rows, branch_width), bf16),
        ((n_tp, branch_width, cols), bf16),
        ((2 * rows, hidden), bf16),
        ((branch_rows, branch_width), bf16),
        ((branch_rows, width), f32),
        ((branch_rows, width), bf16),
        ((rows, cols), bf16),
        ((2, rows, width), f32),
        ((nz, rows, width), bf16),
        ((nz, rows, width), bf16),
        ((nz, 2, nx, ny, qr, cols), bf16),
        ((nz, 2, ny, nx, qr, cols), bf16),
        ((nz, 2, k1, qr, cols), bf16),
        ((nz, 2, ny + nx, qr, cols), bf16),
        ((nz, 2, k2, qr, cols), bf16),
        ((nz, rows, cols), bf16),
        ((nz, rows, cols), bf16),
        ((rows, cols), f32),
    ]
    held = sum(math.prod(shape) * jnp.dtype(kind).itemsize for shape, kind in buffers)
    return pl.pallas_call(
        functools.partial(kernel, n_ep, n_tp),
        out_shape=(
            jax.ShapeDtypeStruct((branch_rows, width), bf16),
            jax.ShapeDtypeStruct((rows, cols), bf16),
        ),
        in_specs=[vm] * 5 + [hbm] * 7,
        out_specs=(anyspace, anyspace),
        scratch_shapes=[pltpu.VMEM(shape, kind) for shape, kind in buffers] + [
            dma((9,)), dma((13,)),
            dma((nz,)), dma((nz,)), dma((nz,)), dma((nz,)), dma((nz,)),
            dma((nz, 2)), dma((nz, 2)), dma((7,)),
        ],
        compiler_params=pltpu.CompilerParams(
            collective_id=0, has_side_effects=True, vmem_limit_bytes=67043328
        ),
    )(
        group_gain.reshape(1, -1), out_gain.reshape(1, -1), ffn_gain.reshape(1, -1), routes.T, route_weight.T,
        branch_in, pool_weight, out_weight, ffn_input, gate_weight, up_weight, down_weight,
    )


def solution(mesh):
    in_specs = (
        P(("ep", "tp"), None),
        P(),
        P(),
        P(None, "tp"),
        P(),
        P("ep", None),
        P(),
        P("ep", None),
        P("ep", None),
        P("ep", None, "tp"),
        P("ep", None, "tp"),
        P("ep", "tp", None),
    )
    out_specs = (P(("ep", "tp"), None), P("ep", "tp"))
    return jax.shard_map(
        functools.partial(per_device, mesh.shape["ep"], mesh.shape["tp"]),
        mesh=mesh, in_specs=in_specs, out_specs=out_specs, check_vma=False,
    )
```

time: 73.2 us -> 61.5 us (0.84)
  Pallas kernels: 67.1 us -> 56.8 us
  other arithmetic: 1.3 us -> 0 us
    pallas_call x1, Pallas kernels: 67.1 us -> 56.8 us  [per_device(): pl.pallas_call(functools.partial(kernel, n_ep, n_tp), out_shape=(jax.Shap...]
    reduce_sum x1 -> x0, other arithmetic: 1.3 us -> none  [per_device(): w_own = jnp.sum(jnp.where(named, route_weight[None, :, :], 0.0), axis=2)]
where the time goes in v1:
time: 61.5 us; the launch traced here: 61.3 us
  Pallas kernels  56.8 us (92%)
  local copies, waits for them, and re-layouts  3.87 us (6%)
  between operations  0.64 us (1%)
    pallas_call x1, Pallas kernels, per_device(): pl.pallas_call(functools.partial(kernel, n_ep, n_tp), out_shape=(jax.Shap...  56.8 us
    unnamed x2, local copies, waits for them, and re-layouts  3.87 us

profile of v1, /device:TPU:0, one launch (start us, length us, event | category | flops | bytes accessed | tf_op | source)
XLA Modules:
  0.0 61.3 jit_solution(2825304582510798094)
XLA Ops:
  0.6 56.8 %shard_map.131 = (bf16[256,2048]{1,0:T(8,128)(2,1)}, bf16[128,512]{1,0:T(8,128)(2,1)}) custom-call(f32[1,512]{1,0:T(1,128)} %bitcast.7, f32[1,2048]{1,0:T(1,128)} %bitcast.5, f32[1,2048]{1,0:T(1,128)} %bitcast.6, s32[4,128]{1,0:T(4,128)} %bitcast.8, f32[4,128]{1,0:T(4,128)} %bitcast.9, bf16[256,512]{1,0:T(8,128)(2,1)} %branch_h.1, ...), custom_call_target="tpu_custom_call" | custom-call | tf_op jit(solution)/shard_map/pallas_call | solution.py:519
  57.4 2.3 %copy.16 = bf16[256,2048]{1,0:T(8,128)(2,1)} copy(bf16[256,2048]{1,0:T(8,128)(2,1)} %get-tuple-element.4) | data formatting | bytes 2097152
  59.7 1.6 %copy.17 = bf16[128,512]{1,0:T(8,128)(2,1)} copy(bf16[128,512]{1,0:T(8,128)(2,1)} %get-tuple-element.5) | data formatting | bytes 262144

commit v2 on v1

--- a/solution.py
+++ b/solution.py
@@ -60,27 +60,28 @@
     S_Z, S_X1, S_X2, S_P, S_W, S_RIM, S_O, S_O2, S_OP, S_M, S_T1, S_T2, S_F = range(13)
     R_W, R_RIM, R_OA, R_OB, R_O2, R_OP, R_F = range(7)
 
+    outer = ((z == 0) | (z == nz - 1)).astype(jnp.int32)
+
     def hop(s):
-        return (nz - s) % nz
-
-    def partner(s, sign):
-        s = hop(s)
+        if isinstance(s, int) and s == 0:
+            return 0
+        turned = s % (nz - 1) + 1
+        return s + outer * jnp.where(s == 0, 0, turned - s)
+
+    def partner(m, sign):
         if not paired:
-            return (z + sign * s + nz) % nz
+            return (z + sign * m + nz) % nz
         total, bit = 0, 1
         while bit < nz:
-            total = total + (z // bit + s // bit) % 2 * bit
+            total = total + (z // bit + m // bit) % 2 * bit
             bit *= 2
         return total
 
-    def ep_at(d):
-        return partner(d, 1) * 2 + c
-
-    def src_ep(d):
-        return partner(d, -1) * 2 + c
-
-    def src_mate(d):
-        return partner(d, -1) * 2 + (1 - c)
+    def src_ep(s):
+        return partner(hop(s), -1) * 2 + c
+
+    def src_mate(s):
+        return partner(hop(s), -1) * 2 + (1 - c)
 
     def at(dy, dx):
         return (y + dy + ny) % ny * nx + (x + dx + nx) % nx
@@ -183,19 +184,26 @@
         view = xg.at[src_ep(d)]
         send(view, view, S_P, r_p.at[d], mate, j)
 
+    def send_block(m):
+        view = xg.at[e, :, colsl(j)]
+        send(view, view, S_Z, r_z.at[m], partner(m, 1) * 2 + c, j)
+
+    def send_rest():
+        pl.when(outer == 0)(lambda: send_block(nz - 1))
+        ow_own(1)
+
     def start_sends():
         load_branch.wait()
         tail = branch.at[pl.ds(branch.shape[0] - rim_rows, rim_rows)]
         send(tail, rim, S_RIM, r_one.at[R_RIM], nxt[0], nxt[1])
         for d in range(1, n_ep):
             send(wg.at[e], wg.at[e], S_W, r_one.at[R_W], (e + d) % n_ep, j)
-        for d in [1, nz - 1] + list(range(2, nz - 1)):
-            view = xg.at[e, :, colsl(j)]
-            send(view, view, S_Z, r_z.at[d], ep_at(d), j)
+        for m in range(1, nz - 1):
+            send_block(m)
+        pl.when(outer == 1)(lambda: send_block(nz - 1))
         to_mate(0)
         own_ow.wait()
         ow_own(0)
-        ow_own(1)
 
     start_sends()
 
@@ -227,7 +235,7 @@
 
     def gather_one(d):
         view = xg.at[src_ep(d), :, colsl(j)]
-        landed(view, r_z.at[d])
+        landed(view, r_z.at[hop(d)])
         for dx in steps_x:
             send(view, view, S_X1, r_x1.at[d], e, at(0, dx))
         for dy in steps_y:
@@ -336,7 +344,7 @@
             fsend[s, top] = a.astype(bf16)
             fsend[s, low] = b.astype(bf16)
             part = pl.ds(2 * h * qr, 2 * qr)
-            send(fsend.at[s, part], frecv.at[s, part], S_F, r_one.at[R_F], src_ep(s), j)
+            send(fsend.at[s, part], frecv.at[hop(s), part], S_F, r_one.at[R_F], src_ep(s), j)
 
     def project():
         landed(ow.at[pl.ds(0, n_tp - 1), pl.ds(0, 2 * quart)], r_one.at[R_OP])
@@ -372,19 +380,19 @@
     plan = {
         0: (
             [(wait_first,)],
-            [],
+            [(send_rest,)],
             [(wait_down,)],
-            [(ow_relay,), (pool,), (G1, 1), (G2, 1), (G1, 2), (G1, 3), (TM, 1)],
+            [(G1, 1), (pool,), (S1, 0, 0), (G2, 1), (G1, 2), (TM, 1), (G1, 3)],
         ),
-        1: ([], [(G2, 2)], [], [(G2, 3), (S1, 1, 0), (S1, 1, 1), (TM, 2)]),
-        2: ([], [(TM, 3), (S1, 0, 0)], [(S2, 1, 0), (S1, 0, 1)], [(S2, 1, 1)]),
+        1: ([], [(G2, 2)], [(ow_relay,)], [(G2, 3), (S1, 1, 0), (TM, 2)]),
+        2: ([], [(S1, 1, 1)], [(S1, 0, 1), (TM, 3)], [(S2, 1, 0), (ow_to_mate,)]),
         end: (
             [],
-            [(S1, end - 1, 0), (ow_to_mate,), (S3, end - 2, 0)],
-            [(S1, end - 1, 1)],
+            [(S1, end - 1, 0)],
+            [(S2, end - 2, 1), (S1, end - 1, 1), (S3, end - 2, 0)],
             [
-                (S3, end - 2, 1), (S2, end - 1, 0), (S1, end, 0), (S2, end - 1, 1), (S1, end, 1),
-                (S3, end - 1, 0), (project,), (S2, end, 0), (S2, 0, 0), (S3, end - 1, 1), (S2, 0, 1),
+                (S2, end - 1, 0), (S3, end - 2, 1), (S1, end, 0), (S2, end - 1, 1), (S1, end, 1),
+                (S3, end - 1, 0), (S2, 0, 0), (project,), (S2, end, 0), (S2, 0, 1), (S3, end - 1, 1),
                 (S2, end, 1), (S3, end, 0), (S3, 0, 0), (S3, end, 1), (S3, 0, 1),
             ],
         ),
@@ -393,15 +401,15 @@
 
     def middle(s, slot):
         if slot == 1:
+            scatter_one(s - 1, 0)
+        if slot == 2:
+            scatter_two(s - 2, 1)
+            scatter_one(s - 1, 1)
+            scatter_end(s - 2, 0)
             to_mate(s + 1)
-            scatter_one(s - 1, 0)
-            scatter_end(s - 2, 0)
-        if slot == 2:
-            scatter_one(s - 1, 1)
         if slot == 3:
+            scatter_two(s - 1, 0)
             scatter_end(s - 2, 1)
-            scatter_two(s - 1, 0)
-            scatter_two(s - 1, 1)
 
     def run(s, slot):
         for i, slots in plan.items():
@@ -515,6 +523,10 @@
         ((nz, rows, cols), bf16),
         ((rows, cols), f32),
     ]
+    operands = (
+        group_gain.reshape(1, -1), out_gain.reshape(1, -1), ffn_gain.reshape(1, -1), routes.T, route_weight.T,
+        branch_in, pool_weight, out_weight, ffn_input, gate_weight, up_weight, down_weight,
+    )
     held = sum(math.prod(shape) * jnp.dtype(kind).itemsize for shape, kind in buffers)
     return pl.pallas_call(
         functools.partial(kernel, n_ep, n_tp),
@@ -530,11 +542,10 @@
             dma((nz, 2)), dma((nz, 2)), dma((7,)),
         ],
         compiler_params=pltpu.CompilerParams(
-            collective_id=0, has_side_effects=True, vmem_limit_bytes=67043328
+            collective_id=0, has_side_effects=True, vmem_limit_bytes=min(67043328, held + (8 << 20))
         ),
     )(
-        group_gain.reshape(1, -1), out_gain.reshape(1, -1), ffn_gain.reshape(1, -1), routes.T, route_weight.T,
-        branch_in, pool_weight, out_weight, ffn_input, gate_weight, up_weight, down_weight,
+        *[pltpu.with_memory_space_constraint(v, pltpu.HBM) for v in operands]
     )
 
 

time: 61.5 us -> 55 us (0.89)
  Pallas kernels: 56.8 us -> 52.5 us
  local copies, waits for them, and re-layouts: 3.87 us -> 1.63 us
    pallas_call x1, Pallas kernels: 56.8 us -> 52.5 us  [per_device(): pl.pallas_call(functools.partial(kernel, n_ep, n_tp), out_shape=(jax.Shap...]
    unnamed x2, local copies, waits for them, and re-layouts: 3.87 us -> 1.63 us
where the time goes in v2:
time: 55 us; the launch traced here: 54.7 us
  Pallas kernels  52.5 us (95%)
  local copies, waits for them, and re-layouts  1.63 us (3%)
  between operations  0.64 us (1%)
    pallas_call x1, Pallas kernels, per_device(): pl.pallas_call(functools.partial(kernel, n_ep, n_tp), out_shape=(jax.Shap...  52.5 us
    unnamed x2, local copies, waits for them, and re-layouts  1.63 us

profile of v2, /device:TPU:0, one launch (start us, length us, event | category | flops | bytes accessed | tf_op | source)
XLA Modules:
  0.0 54.7 jit_solution(8730590846542620456)
XLA Ops:
  0.6 52.5 %shard_map.131 = (bf16[256,2048]{1,0:T(8,128)(2,1)S(1)}, bf16[128,512]{1,0:T(8,128)(2,1)S(1)}) custom-call(f32[1,512]{1,0:T(1,128)} %bitcast.7, f32[1,2048]{1,0:T(1,128)} %bitcast.5, f32[1,2048]{1,0:T(1,128)} %bitcast.6, s32[4,128]{1,0:T(4,128)} %bitcast.8, f32[4,128]{1,0:T(4,128)} %bitcast.9, bf16[256,512]{1,0:T(8,128)(2,1)} %branch_h.1, ...), custom_call_target="tpu_custom_call" | custom-call | tf_op jit(solution)/shard_map/pallas_call | solution.py:531
  53.1 1.0 %copy.16 = bf16[256,2048]{1,0:T(8,128)(2,1)} copy(bf16[256,2048]{1,0:T(8,128)(2,1)S(1)} %get-tuple-element.4) | data formatting | bytes 2097152
  54.1 0.7 %copy.17 = bf16[128,512]{1,0:T(8,128)(2,1)} copy(bf16[128,512]{1,0:T(8,128)(2,1)S(1)} %get-tuple-element.5) | data formatting | bytes 262144

commit v3 on v2

--- a/solution.py
+++ b/solution.py
@@ -31,9 +31,10 @@
 
 def kernel(
     n_ep, n_tp,
-    group_gain, out_gain, ffn_gain, routes, route_w, branch_h, pool_h, out_w, x_h, gate_h, up_h, down_h,
+    group_gain_h, out_gain_h, ffn_gain_h, routes_h, route_w_h, branch_h, pool_h, out_w, x_h,
+    gate_h, up_h, down_h,
     mixer_h, expert_h,
-    branch, pool_w, x_own, gate, up, down, xg, wg, rim, ow, hid, mixed, proj, mixer_out, expert_out,
+    group_gain, out_gain, ffn_gain, routes, route_w, branch, pool_w, x_own, gate, up, down, xg, wg, rim, ow, hid, mixed, proj, mixer_out, expert_out,
     pown, psend, precv, ts_a, ts_b, t1, u2, t2, fsend, frecv, facc,
     local_sem, sent, r_z, r_x1, r_x2, r_p, r_m, r_t1, r_t2, r_one,
 ):
@@ -122,7 +123,16 @@
     ]
     write_mixer = pltpu.make_async_copy(mixer_out, mixer_h, local_sem.at[7])
     write_expert = pltpu.make_async_copy(expert_out, expert_h, local_sem.at[8])
-    for load in [load_x, load_branch, own_ow, load_pool] + loads:
+    load_gain = pltpu.make_async_copy(ffn_gain_h, ffn_gain, local_sem.at[9])
+    load_route = [
+        pltpu.make_async_copy(routes_h, routes, local_sem.at[10]),
+        pltpu.make_async_copy(route_w_h, route_w, local_sem.at[11]),
+    ]
+    load_late = [
+        pltpu.make_async_copy(group_gain_h, group_gain, local_sem.at[12]),
+        pltpu.make_async_copy(out_gain_h, out_gain, local_sem.at[13]),
+    ]
+    for load in [load_x, load_gain] + load_route + [own_ow, load_branch] + loads + [load_pool] + load_late:
         load.start()
 
     chunk = 16
@@ -132,13 +142,15 @@
         xg[e, r, :] = rms_scale(x_own[r, :].astype(f32), ffn_gain[...]).astype(bf16)
         return 0
 
-    experts = lax.broadcasted_iota(jnp.int32, (n_ep, rows), 0)
-    named = jnp.zeros((n_ep, rows), f32)
-    for k in range(routes.shape[0]):
-        named = named + jnp.where(routes[pl.ds(k, 1), :] == experts, route_w[pl.ds(k, 1), :], 0.0)
-    wg[e] = named
-
     def norm_part():
+        for load in load_route:
+            load.wait()
+        experts = lax.broadcasted_iota(jnp.int32, (n_ep, rows), 0)
+        named = jnp.zeros((n_ep, rows), f32)
+        for k in range(routes.shape[0]):
+            named = named + jnp.where(routes[pl.ds(k, 1), :] == experts, route_w[pl.ds(k, 1), :], 0.0)
+        wg[e] = named
+        load_gain.wait()
         load_x.wait()
         lax.fori_loop(0, rows // chunk, norm_rows, 0)
 
@@ -190,7 +202,6 @@
 
     def send_rest():
         pl.when(outer == 0)(lambda: send_block(nz - 1))
-        ow_own(1)
 
     def start_sends():
         load_branch.wait()
@@ -204,6 +215,7 @@
         to_mate(0)
         own_ow.wait()
         ow_own(0)
+        ow_own(1)
 
     start_sends()
 
@@ -211,6 +223,8 @@
 
     def pool():
         load_pool.wait()
+        for load in load_late:
+            load.wait()
         landed(rim, r_one.at[R_RIM])
         chans = branch.shape[1] // len(pool_windows)
         first_row = (e * n_tp + j) * branch_rows
@@ -381,19 +395,19 @@
         0: (
             [(wait_first,)],
             [(send_rest,)],
-            [(wait_down,)],
-            [(G1, 1), (pool,), (S1, 0, 0), (G2, 1), (G1, 2), (TM, 1), (G1, 3)],
+            [(G1, 1), (wait_down,)],
+            [(S1, 0, 0), (G2, 1), (G1, 2), (G1, 3), (pool,), (TM, 1)],
         ),
-        1: ([], [(G2, 2)], [(ow_relay,)], [(G2, 3), (S1, 1, 0), (TM, 2)]),
-        2: ([], [(S1, 1, 1)], [(S1, 0, 1), (TM, 3)], [(S2, 1, 0), (ow_to_mate,)]),
+        1: ([], [(G2, 2), (S1, 0, 1)], [], [(G2, 3), (S2, 0, 0), (TM, 2), (S1, 1, 0), (S1, 1, 1)]),
+        2: ([], [], [(TM, 3), (ow_relay,)], [(S2, 1, 0)]),
         end: (
             [],
-            [(S1, end - 1, 0)],
-            [(S2, end - 2, 1), (S1, end - 1, 1), (S3, end - 2, 0)],
+            [(S1, end - 1, 0), (S2, end - 2, 1), (S1, end - 1, 1)],
+            [],
             [
-                (S2, end - 1, 0), (S3, end - 2, 1), (S1, end, 0), (S2, end - 1, 1), (S1, end, 1),
-                (S3, end - 1, 0), (S2, 0, 0), (project,), (S2, end, 0), (S2, 0, 1), (S3, end - 1, 1),
-                (S2, end, 1), (S3, end, 0), (S3, 0, 0), (S3, end, 1), (S3, 0, 1),
+                (S2, end - 1, 0), (S3, end - 2, 0), (S3, end - 2, 1), (S1, end, 0), (S2, end - 1, 1),
+                (S1, end, 1), (ow_to_mate,), (S3, end - 1, 0), (S2, end, 0), (S3, end - 1, 1), (S2, end, 1),
+                (S2, 0, 1), (S3, 0, 0), (S3, end, 0), (project,), (S3, end, 1), (S3, 0, 1),
             ],
         ),
     }
@@ -402,13 +416,13 @@
     def middle(s, slot):
         if slot == 1:
             scatter_one(s - 1, 0)
-        if slot == 2:
             scatter_two(s - 2, 1)
             scatter_one(s - 1, 1)
-            scatter_end(s - 2, 0)
+        if slot == 2:
             to_mate(s + 1)
         if slot == 3:
             scatter_two(s - 1, 0)
+            scatter_end(s - 2, 0)
             scatter_end(s - 2, 1)
 
     def run(s, slot):
@@ -489,13 +503,17 @@
     qr = rows // 4
     hidden = gate_weight.shape[2]
     branch_rows, branch_width = branch_in.shape
-    vm = pl.BlockSpec(memory_space=pltpu.VMEM)
     hbm = pl.BlockSpec(memory_space=pltpu.HBM)
     anyspace = pl.BlockSpec(memory_space=pl.ANY)
     dma = pltpu.SemaphoreType.DMA
     k1 = (nx - 1) * ny + (ny - 1) * nx
     k2 = nx + ny - 2
     buffers = [
+        ((1, branch_width), f32),
+        ((1, width), f32),
+        ((1, width), f32),
+        (routes.shape[::-1], jnp.int32),
+        (route_weight.shape[::-1], f32),
         ((branch_rows, branch_width), bf16),
         (pool_weight.shape, bf16),
         ((rows, width), bf16),
@@ -534,10 +552,10 @@
             jax.ShapeDtypeStruct((branch_rows, width), bf16),
             jax.ShapeDtypeStruct((rows, cols), bf16),
         ),
-        in_specs=[vm] * 5 + [hbm] * 7,
+        in_specs=[hbm] * 12,
         out_specs=(anyspace, anyspace),
         scratch_shapes=[pltpu.VMEM(shape, kind) for shape, kind in buffers] + [
-            dma((9,)), dma((13,)),
+            dma((14,)), dma((13,)),
             dma((nz,)), dma((nz,)), dma((nz,)), dma((nz,)), dma((nz,)),
             dma((nz, 2)), dma((nz, 2)), dma((7,)),
         ],

time: 55 us -> 53.9 us (0.980)
  Pallas kernels: 52.5 us -> 51.3 us
    pallas_call x1, Pallas kernels: 52.5 us -> 51.3 us  [per_device(): pl.pallas_call(functools.partial(kernel, n_ep, n_tp), out_shape=(jax.Shap...]
where the time goes in v3:
time: 53.9 us; the launch traced here: 53.5 us
  Pallas kernels  51.3 us (95%)
  local copies, waits for them, and re-layouts  1.63 us (3%)
  between operations  0.64 us (1%)
    pallas_call x1, Pallas kernels, per_device(): pl.pallas_call(functools.partial(kernel, n_ep, n_tp), out_shape=(jax.Shap...  51.3 us
    unnamed x2, local copies, waits for them, and re-layouts  1.63 us

profile of v3, /device:TPU:0, one launch (start us, length us, event | category | flops | bytes accessed | tf_op | source)
XLA Modules:
  0.0 53.5 jit_solution(4205909834197613904)
XLA Ops:
  0.6 51.3 %shard_map.131 = (bf16[256,2048]{1,0:T(8,128)(2,1)S(1)}, bf16[128,512]{1,0:T(8,128)(2,1)S(1)}) custom-call(f32[1,512]{1,0:T(1,128)} %bitcast.7, f32[1,2048]{1,0:T(1,128)} %bitcast.5, f32[1,2048]{1,0:T(1,128)} %bitcast.6, s32[4,128]{1,0:T(4,128)} %bitcast.8, f32[4,128]{1,0:T(4,128)} %bitcast.9, bf16[256,512]{1,0:T(8,128)(2,1)} %branch_h.1, ...), custom_call_target="tpu_custom_call" | custom-call | tf_op jit(solution)/shard_map/pallas_call | solution.py:549
  51.9 1.0 %copy.16 = bf16[256,2048]{1,0:T(8,128)(2,1)} copy(bf16[256,2048]{1,0:T(8,128)(2,1)S(1)} %get-tuple-element.4) | data formatting | bytes 2097152
  52.9 0.7 %copy.17 = bf16[128,512]{1,0:T(8,128)(2,1)} copy(bf16[128,512]{1,0:T(8,128)(2,1)S(1)} %get-tuple-element.5) | data formatting | bytes 262144

commit v4 on v3

--- a/solution.py
+++ b/solution.py
@@ -58,8 +58,8 @@
     nxt = ((e + last) % n_ep, (j + 1) % n_tp)
     prv = ((e - first + n_ep) % n_ep, (j - 1 + n_tp) % n_tp)
     paired = nz & (nz - 1) == 0
-    S_Z, S_X1, S_X2, S_P, S_W, S_RIM, S_O, S_O2, S_OP, S_M, S_T1, S_T2, S_F = range(13)
-    R_W, R_RIM, R_OA, R_OB, R_O2, R_OP, R_F = range(7)
+    S_Z, S_X1, S_X2, S_P, S_W, S_RIM, S_O, S_O2, S_OP, S_M, S_T1, S_T2, S_F, S_OZ = range(14)
+    R_W, R_RIM, R_OA, R_OB, R_O2, R_OP, R_F, R_OZ = range(8)
 
     outer = ((z == 0) | (z == nz - 1)).astype(jnp.int32)
 
@@ -160,8 +160,11 @@
     norm_part()
     barrier_wait()
 
-    quart = out_w.shape[0] // 4
-    ow_rows = [pl.ds(pl.multiple_of((c * 2 + k) * quart, quart), quart) for k in range(2)]
+    eighth = out_w.shape[0] // 8
+    quart = 2 * eighth
+    share = (c * 2 + z % 2) * quart
+    ow_rows = [pl.ds(pl.multiple_of(share + k * eighth, eighth), eighth) for k in range(2)]
+    my_quart = pl.ds(pl.multiple_of(share, quart), quart)
     my_half = pl.ds(pl.multiple_of(c * 2 * quart, quart), 2 * quart)
 
     def ow_own(k):
@@ -173,7 +176,7 @@
             send(mine, mine, S_O, r_one.at[R_OA + k], e, at(dy, 0))
 
     def ow_relay():
-        landed(ow.at[pl.ds(0, near), pl.ds(0, quart)], r_one.at[R_OA])
+        landed(ow.at[pl.ds(0, near), pl.ds(0, eighth)], r_one.at[R_OA])
         for dx in steps_x:
             view = ow.at[at(0, -dx), ow_rows[0]]
             for dy in steps_y:
@@ -183,18 +186,25 @@
             for dx in steps_x:
                 send(view, view, S_O2, r_one.at[R_O2], e, at(0, dx))
 
+    def ow_along_z():
+        landed(ow.at[pl.ds(0, near), pl.ds(0, eighth)], r_one.at[R_OB])
+        landed(ow.at[pl.ds(0, far), pl.ds(0, quart)], r_one.at[R_O2])
+        for t in range(1, n_tp):
+            view = ow.at[(j + t) % n_tp, my_quart]
+            send(view, view, S_OZ, r_one.at[R_OZ], (z + 1 - z % 2 * 2) * 2 + c, j)
+
     def ow_to_mate():
-        landed(ow.at[pl.ds(0, near), pl.ds(0, quart)], r_one.at[R_OB])
-        landed(ow.at[pl.ds(0, far), pl.ds(0, 2 * quart)], r_one.at[R_O2])
+        landed(ow.at[pl.ds(0, n_tp - 1), pl.ds(0, quart)], r_one.at[R_OZ])
         for t in range(1, n_tp):
             view = ow.at[(j + t) % n_tp, my_half]
             send(view, view, S_OP, r_one.at[R_OP], mate, j)
 
-    def to_mate(d):
-        if not (isinstance(d, int) and d == 0):
-            landed(xg.at[0, :, pl.ds(0, far * cols)], r_x2.at[d])
-        view = xg.at[src_ep(d)]
+    def to_mate(d, rows_at, q):
+        view = xg.at[src_ep(d), rows_at, colsl(q)]
         send(view, view, S_P, r_p.at[d], mate, j)
+
+    def own_to_mate():
+        send(xg.at[e], xg.at[e], S_P, r_p.at[0], mate, j)
 
     def send_block(m):
         view = xg.at[e, :, colsl(j)]
@@ -212,7 +222,7 @@
         for m in range(1, nz - 1):
             send_block(m)
         pl.when(outer == 1)(lambda: send_block(nz - 1))
-        to_mate(0)
+        own_to_mate()
         own_ow.wait()
         ow_own(0)
         ow_own(1)
@@ -248,15 +258,18 @@
         mixed[...] = (proj[:, : branch.shape[1]] * scale * group_gain[...]).astype(bf16)
 
     def gather_one(d):
-        view = xg.at[src_ep(d), :, colsl(j)]
-        landed(view, r_z.at[hop(d)])
-        for dx in steps_x:
-            send(view, view, S_X1, r_x1.at[d], e, at(0, dx))
-        for dy in steps_y:
-            send(view, view, S_X1, r_x1.at[d], e, at(dy, 0))
+        whole = xg.at[src_ep(d), :, colsl(j)]
+        landed(whole, r_z.at[hop(d)])
+        parts = [xg.at[src_ep(d), r, colsl(j)] for r in (upper, lower)]
+        for k in range(2):
+            for dx in steps_x:
+                send(parts[k], parts[k], S_X1, r_x1.at[d, k], e, at(0, dx))
+            for dy in steps_y:
+                send(parts[1 - k], parts[1 - k], S_X1, r_x1.at[d, k], e, at(dy, 0))
+        to_mate(d, pl.ds(0, rows), j)
 
     def gather_two(d):
-        landed(xg.at[0, :, pl.ds(0, near * cols)], r_x1.at[d])
+        landed(xg.at[0, upper, pl.ds(0, near * cols)], r_x1.at[d, 0])
         for dx in steps_x:
             view = xg.at[src_ep(d), upper, colsl(at(0, -dx))]
             for dy in steps_y:
@@ -265,6 +278,21 @@
             view = xg.at[src_ep(d), lower, colsl(at(-dy, 0))]
             for dx in steps_x:
                 send(view, view, S_X2, r_x2.at[d], e, at(0, dx))
+        for dx in steps_x:
+            to_mate(d, upper, at(0, -dx))
+        for dy in steps_y:
+            to_mate(d, lower, at(-dy, 0))
+
+    def gather_end(d):
+        landed(xg.at[0, upper, pl.ds(0, near * cols)], r_x1.at[d, 1])
+        for dx in steps_x:
+            to_mate(d, lower, at(0, -dx))
+        for dy in steps_y:
+            to_mate(d, upper, at(-dy, 0))
+        landed(xg.at[0, :, pl.ds(0, far * cols)], r_x2.at[d])
+        for dx in steps_x:
+            for dy in steps_y:
+                to_mate(d, pl.ds(0, rows), at(-dy, -dx))
 
     diagonal = lax.broadcasted_iota(jnp.int32, (rows, rows), 0) == lax.broadcasted_iota(
         jnp.int32, (rows, rows), 1
@@ -389,37 +417,42 @@
         loads[2].wait()
         landed(wg.at[pl.ds(0, n_ep - 1)], r_one.at[R_W])
 
-    G1, G2, TM, S1, S2, S3 = gather_one, gather_two, to_mate, scatter_one, scatter_two, scatter_end
+    G1, G2, TM, S1, S2, S3 = gather_one, gather_two, gather_end, scatter_one, scatter_two, scatter_end
     end = nz - 1
     plan = {
         0: (
             [(wait_first,)],
-            [(send_rest,)],
+            [(send_rest,), (ow_relay,)],
             [(G1, 1), (wait_down,)],
-            [(S1, 0, 0), (G2, 1), (G1, 2), (G1, 3), (pool,), (TM, 1)],
+            [(G2, 1), (G1, 2), (ow_along_z,), (TM, 1), (S1, 0, 0)],
         ),
-        1: ([], [(G2, 2), (S1, 0, 1)], [], [(G2, 3), (S2, 0, 0), (TM, 2), (S1, 1, 0), (S1, 1, 1)]),
-        2: ([], [], [(TM, 3), (ow_relay,)], [(S2, 1, 0)]),
+        1: (
+            [],
+            [(G2, 2), (G1, 3)],
+            [],
+            [(TM, 2), (G2, 3), (S1, 1, 0), (pool,), (S1, 1, 1), (S2, 0, 0)],
+        ),
+        2: ([], [], [(S1, 0, 1), (TM, 3)], [(S2, 1, 0)]),
         end: (
             [],
-            [(S1, end - 1, 0), (S2, end - 2, 1), (S1, end - 1, 1)],
-            [],
+            [(S1, end - 1, 0)],
+            [(S2, end - 2, 1), (S1, end - 1, 1)],
             [
-                (S2, end - 1, 0), (S3, end - 2, 0), (S3, end - 2, 1), (S1, end, 0), (S2, end - 1, 1),
-                (S1, end, 1), (ow_to_mate,), (S3, end - 1, 0), (S2, end, 0), (S3, end - 1, 1), (S2, end, 1),
-                (S2, 0, 1), (S3, 0, 0), (S3, end, 0), (project,), (S3, end, 1), (S3, 0, 1),
+                (S3, 0, 0), (S2, end - 1, 0), (S3, end - 2, 0), (S3, end - 2, 1), (S1, end, 0),
+                (S2, end - 1, 1), (S1, end, 1), (ow_to_mate,), (S3, end - 1, 0), (S2, 0, 1), (S2, end, 0),
+                (S3, end - 1, 1), (S2, end, 1), (S3, 0, 1), (S3, end, 0), (S3, end, 1), (project,),
             ],
         ),
     }
-    assert nz >= 4
+    assert nz >= 4 and nz % 2 == 0
 
     def middle(s, slot):
         if slot == 1:
             scatter_one(s - 1, 0)
+        if slot == 2:
             scatter_two(s - 2, 1)
             scatter_one(s - 1, 1)
-        if slot == 2:
-            to_mate(s + 1)
+            gather_end(s + 1)
         if slot == 3:
             scatter_two(s - 1, 0)
             scatter_end(s - 2, 0)
@@ -460,15 +493,15 @@
     lax.fori_loop(0, nz, step, 0)
 
     def drain_all():
-        write_mixer.wait()
         landed(fsend.at[pl.ds(1, nz - 1)], sent.at[S_Z])
         landed(xg.at[pl.ds(0, nz - 1), :, pl.ds(0, near * cols)], sent.at[S_X1])
         landed(xg.at[pl.ds(0, nz - 1), :, pl.ds(0, far * cols)], sent.at[S_X2])
         landed(psend, sent.at[S_P])
         landed(wg.at[pl.ds(0, n_ep - 1)], sent.at[S_W])
         landed(rim, sent.at[S_RIM])
-        landed(ow.at[pl.ds(0, near), pl.ds(0, 2 * quart)], sent.at[S_O])
-        landed(ow.at[pl.ds(0, far), pl.ds(0, 2 * quart)], sent.at[S_O2])
+        landed(ow.at[pl.ds(0, near), pl.ds(0, quart)], sent.at[S_O])
+        landed(ow.at[pl.ds(0, far), pl.ds(0, quart)], sent.at[S_O2])
+        landed(ow.at[pl.ds(0, n_tp - 1), pl.ds(0, quart)], sent.at[S_OZ])
         landed(ow.at[pl.ds(0, n_tp - 1), pl.ds(0, 2 * quart)], sent.at[S_OP])
         landed(psend, sent.at[S_M])
         landed(t1, sent.at[S_T1])
@@ -483,6 +516,7 @@
 
     def finish():
         write_expert.start()
+        write_mixer.wait()
         landed(fsend.at[pl.ds(1, nz - 1)], sent.at[S_F])
         write_expert.wait()
 
@@ -555,9 +589,9 @@
         in_specs=[hbm] * 12,
         out_specs=(anyspace, anyspace),
         scratch_shapes=[pltpu.VMEM(shape, kind) for shape, kind in buffers] + [
-            dma((14,)), dma((13,)),
-            dma((nz,)), dma((nz,)), dma((nz,)), dma((nz,)), dma((nz,)),
-            dma((nz, 2)), dma((nz, 2)), dma((7,)),
+            dma((14,)), dma((14,)),
+            dma((nz,)), dma((nz, 2)), dma((nz,)), dma((nz,)), dma((nz,)),
+            dma((nz, 2)), dma((nz, 2)), dma((8,)),
         ],
         compiler_params=pltpu.CompilerParams(
             collective_id=0, has_side_effects=True, vmem_limit_bytes=min(67043328, held + (8 << 20))

time: 53.9 us -> 52.9 us (0.981)
  Pallas kernels: 51.3 us -> 50 us
    pallas_call x1, Pallas kernels: 51.3 us -> 50 us  [per_device(): pl.pallas_call(functools.partial(kernel, n_ep, n_tp), out_shape=(jax.Shap...]
where the time goes in v4:
time: 52.9 us; the launch traced here: 52.3 us
  Pallas kernels  50 us (95%)
  local copies, waits for them, and re-layouts  1.63 us (3%)
  between operations  0.64 us (1%)
    pallas_call x1, Pallas kernels, per_device(): pl.pallas_call(functools.partial(kernel, n_ep, n_tp), out_shape=(jax.Shap...  50 us
    unnamed x2, local copies, waits for them, and re-layouts  1.63 us

profile of v4, /device:TPU:0, one launch (start us, length us, event | category | flops | bytes accessed | tf_op | source)
XLA Modules:
  0.0 52.3 jit_solution(16429943325020130810)
XLA Ops:
  0.6 50.0 %shard_map.131 = (bf16[256,2048]{1,0:T(8,128)(2,1)S(1)}, bf16[128,512]{1,0:T(8,128)(2,1)S(1)}) custom-call(f32[1,512]{1,0:T(1,128)} %bitcast.7, f32[1,2048]{1,0:T(1,128)} %bitcast.5, f32[1,2048]{1,0:T(1,128)} %bitcast.6, s32[4,128]{1,0:T(4,128)} %bitcast.8, f32[4,128]{1,0:T(4,128)} %bitcast.9, bf16[256,512]{1,0:T(8,128)(2,1)} %branch_h.1, ...), custom_call_target="tpu_custom_call" | custom-call | tf_op jit(solution)/shard_map/pallas_call | solution.py:583
  50.7 1.0 %copy.16 = bf16[256,2048]{1,0:T(8,128)(2,1)} copy(bf16[256,2048]{1,0:T(8,128)(2,1)S(1)} %get-tuple-element.4) | data formatting | bytes 2097152
  51.7 0.7 %copy.17 = bf16[128,512]{1,0:T(8,128)(2,1)} copy(bf16[128,512]{1,0:T(8,128)(2,1)S(1)} %get-tuple-element.5) | data formatting | bytes 262144

commit v5 on v4

--- a/solution.py
+++ b/solution.py
@@ -314,21 +314,14 @@
         u = jnp.clip(u, -clamp_limit, clamp_limit)
         hid[:, span] = ((u + 1.0) * g * jax.nn.sigmoid(sigmoid_slope * g)).astype(bf16)
 
-    step_d = min(1024, width)
-
     def down_part(s):
+        theirs = row_weights(src_mate(s))
         mine = row_weights(src_ep(s))
-        theirs = row_weights(src_mate(s))
-
-        def one(q, _):
-            span = pl.ds(pl.multiple_of(q * step_d, step_d), step_d)
-            out = jnp.dot(hid[...], down[:, span], preferred_element_type=f32)
-            psend[s, :, span] = (out[rows:] * theirs).astype(bf16)
-            pown[s % 2, :, span] = out[:rows] * mine
-            send(psend.at[s, :, span], precv.at[s, :, span], S_M, r_m.at[s], mate, j)
-            return 0
-
-        lax.fori_loop(0, width // step_d, one, 0)
+        out = jnp.dot(hid[rows:], down[...], preferred_element_type=f32)
+        psend[s] = (out * theirs).astype(bf16)
+        send(psend.at[s], precv.at[s], S_M, r_m.at[s], mate, j)
+        out = jnp.dot(hid[:rows], down[...], preferred_element_type=f32)
+        pown[s % 2] = out * mine
 
     def scatter_one(s, h):
         if h == 0:
@@ -422,15 +415,15 @@
     plan = {
         0: (
             [(wait_first,)],
-            [(send_rest,), (ow_relay,)],
+            [(ow_relay,)],
             [(G1, 1), (wait_down,)],
-            [(G2, 1), (G1, 2), (ow_along_z,), (TM, 1), (S1, 0, 0)],
+            [(send_rest,), (G2, 1), (G1, 2), (ow_along_z,), (pool,), (TM, 1), (S1, 0, 0)],
         ),
         1: (
             [],
             [(G2, 2), (G1, 3)],
             [],
-            [(TM, 2), (G2, 3), (S1, 1, 0), (pool,), (S1, 1, 1), (S2, 0, 0)],
+            [(TM, 2), (G2, 3), (S1, 1, 0), (S1, 1, 1), (S2, 0, 0)],
         ),
         2: ([], [], [(S1, 0, 1), (TM, 3)], [(S2, 1, 0)]),
         end: (
@@ -439,7 +432,7 @@
             [(S2, end - 2, 1), (S1, end - 1, 1)],
             [
                 (S3, 0, 0), (S2, end - 1, 0), (S3, end - 2, 0), (S3, end - 2, 1), (S1, end, 0),
-                (S2, end - 1, 1), (S1, end, 1), (ow_to_mate,), (S3, end - 1, 0), (S2, 0, 1), (S2, end, 0),
+                (S1, end, 1), (S2, end - 1, 1), (ow_to_mate,), (S3, end - 1, 0), (S2, 0, 1), (S2, end, 0),
                 (S3, end - 1, 1), (S2, end, 1), (S3, 0, 1), (S3, end, 0), (S3, end, 1), (project,),
             ],
         ),

time: 52.9 us -> 52.4 us (level)
  no operation moved by 1% of the time
where the time goes in v5:
time: 52.4 us; the launch traced here: 52.3 us
  Pallas kernels  50 us (95%)
  local copies, waits for them, and re-layouts  1.63 us (3%)
  between operations  0.64 us (1%)
    pallas_call x1, Pallas kernels, per_device(): pl.pallas_call(functools.partial(kernel, n_ep, n_tp), out_shape=(jax.Shap...  50 us
    unnamed x2, local copies, waits for them, and re-layouts  1.63 us

profile of v5, /device:TPU:0, one launch (start us, length us, event | category | flops | bytes accessed | tf_op | source)
XLA Modules:
  0.0 52.3 jit_solution(1621454648385478185)
XLA Ops:
  0.6 50.0 %shard_map.131 = (bf16[256,2048]{1,0:T(8,128)(2,1)S(1)}, bf16[128,512]{1,0:T(8,128)(2,1)S(1)}) custom-call(f32[1,512]{1,0:T(1,128)} %bitcast.7, f32[1,2048]{1,0:T(1,128)} %bitcast.5, f32[1,2048]{1,0:T(1,128)} %bitcast.6, s32[4,128]{1,0:T(4,128)} %bitcast.8, f32[4,128]{1,0:T(4,128)} %bitcast.9, bf16[256,512]{1,0:T(8,128)(2,1)} %branch_h.1, ...), custom_call_target="tpu_custom_call" | custom-call | tf_op jit(solution)/shard_map/pallas_call | solution.py:576
  50.6 1.0 %copy.16 = bf16[256,2048]{1,0:T(8,128)(2,1)} copy(bf16[256,2048]{1,0:T(8,128)(2,1)S(1)} %get-tuple-element.4) | data formatting | bytes 2097152
  51.6 0.7 %copy.17 = bf16[128,512]{1,0:T(8,128)(2,1)} copy(bf16[128,512]{1,0:T(8,128)(2,1)S(1)} %get-tuple-element.5) | data formatting | bytes 262144
